TPU v7x, 128 devices: a whole 4x4x4 slice. The times are simulated.
128 devices in a mesh: ep: 32 (over z, y, core), tp: 4 (over x).
Axes of the slice: x: 4, y: 4, z: 4, core: 2. Of those that a mesh axis runs over, the one named last changes fastest.
Arguments:
- tokens: bfloat16 [16384, 2048], P(('ep', 'tp')), may hold values from -6 to 6
- norm_gain: float32 [2048], replicated, may hold values from 0.1 to 1.9
- w_gate: bfloat16 [128, 2048, 512], P(('ep', 'tp')), may hold values from -0.125 to 0.125
- w_up: bfloat16 [128, 2048, 512], P(('ep', 'tp')), may hold values from -0.125 to 0.125
- w_down: bfloat16 [128, 512, 2048], P(('ep', 'tp')), may hold values from -0.25 to 0.25
- routing: int32 [16384, 2], P(('ep', 'tp')), may hold values from 0 to 127, as said below
- gate_weight: float32 [16384, 2], P(('ep', 'tp')), may hold values from 0.05 to 1
Outputs:
- combined: bfloat16 [16384, 2048], P(('ep', 'tp'))
Inputs may be any that keep to these rules, and one draw needn't show every extreme that they name: `routing`: A token's 2 experts are distinct and lie in one group of 4 consecutive experts. Of the 128 tokens of each device exactly 4 choose each group; no expert is named by more than 4 tokens of one device, and in every group one expert is named by exactly 4 tokens of every device.
All inputs are finite; a program needn't handle non-finite values.
Results may differ from a plain program's by a relative error of at most 0.0085.
Values may be sent and summed in bfloat16 or wider, within the bound.
A program may use at most 64 MiB of HBM per device.

v0:
```python
import jax
import jax.numpy as jnp
from jax import lax
from jax.sharding import PartitionSpec as P


def local(tokens, norm_gain, w_gate, w_up, w_down, routing, gate_weight):
    tok_rows, width = tokens.shape
    ep_count = lax.axis_size("ep")
    tp_count = lax.axis_size("tp")
    experts = ep_count * tp_count
    capacity = 4 * tok_rows // experts
    values = tokens.astype(jnp.float32)
    scale = lax.rsqrt(jnp.mean(values * values, axis=-1, keepdims=True) + 1e-06)
    normed = (values * scale * norm_gain).astype(jnp.bfloat16)
    normed_pad = jnp.concatenate([normed, jnp.zeros((1, width), jnp.bfloat16)], axis=0)
    assigned = routing.reshape(-1)
    onehot = (assigned[:, None] == jnp.arange(experts, dtype=jnp.int32)[None, :]).astype(jnp.int32)
    running = jnp.cumsum(onehot, axis=0)
    slot_index = jnp.sum(onehot * running, axis=1) - 1
    position = assigned * capacity + slot_index
    slot_owner = jnp.full((experts * capacity,), tok_rows, jnp.int32)
    slot_owner = slot_owner.at[position].set(
        jnp.arange(assigned.shape[0], dtype=jnp.int32) // routing.shape[1]
    )
    outgoing = normed_pad[slot_owner].reshape(experts, capacity, width)
    arrived = lax.all_to_all(outgoing, ("ep", "tp"), split_axis=0, concat_axis=0, tiled=True)
    slot_rows = arrived.reshape(-1, width)
    gate_part = jnp.dot(slot_rows, w_gate[0], preferred_element_type=jnp.float32)
    up_part = jnp.dot(slot_rows, w_up[0], preferred_element_type=jnp.float32)
    hidden = (jax.nn.silu(gate_part) * up_part).astype(jnp.bfloat16)
    expert_out = jnp.dot(hidden, w_down[0], preferred_element_type=jnp.float32).astype(jnp.bfloat16)
    answered = expert_out.reshape(arrived.shape)
    returned = lax.all_to_all(answered, ("ep", "tp"), split_axis=0, concat_axis=0, tiled=True)
    picked = returned.reshape(experts * capacity, width)[position]
    picked = picked.reshape(tok_rows, routing.shape[1], width).astype(jnp.float32)
    combined = jnp.sum(gate_weight[:, :, None] * picked, axis=1)
    return combined.astype(jnp.bfloat16)


def solution(mesh):
    placed = (
        P(("ep", "tp"), None),
        P(),
        P(("ep", "tp"), None, None),
        P(("ep", "tp"), None, None),
        P(("ep", "tp"), None, None),
        P(("ep", "tp"), None),
        P(("ep", "tp"), None),
    )
    return jax.shard_map(
        local, mesh=mesh, in_specs=placed, out_specs=P(("ep", "tp"), None), check_vma=False
    )
```

profile of v0, /device:TPU:1, one launch (start us, length us, event | category | flops | bytes accessed | tf_op | source)
XLA Modules:
  0.0 126.6 jit_solution(14652439876208420146)
XLA Ops:
  0.0 0.0 copy-start
  0.0 0.0 copy-start.1
  0.0 0.9 copy.11
  0.9 0.1 eq.29
  1.1 0.1 eq.25
  1.2 0.7 broadcast_multiply_fusion
  1.9 0.1 copy.13
  2.0 0.2 fusion.17
  2.3 0.2 fusion.18
  2.5 0.1 copy.10
  2.6 0.1 mul.61
  2.8 1.4 %scatter_custom_fusion = s32[512]{0:T(512)S(1)} fusion(s32[256]{0:T(256)S(1)} %bitcast.33, s32[256]{0:T(256)S(1)} %and_select_fusion, s32[]{:T(128)} %constant.37.clone.1), kind=kCustom, calls=%fused_computation.35 | custom fusion | bytes 2052 | tf_op jit(solution)/shard_map/scatter | solution.py:23
  4.2 1.2 fusion.11
  5.5 0.0 copy-done.1
  5.5 0.9 fusion.13
  6.4 3.3 %gather_fusion = bf16[512,2048]{1,0:T(8,128)(2,1)} fusion(bf16[129,2048]{1,0:T(8,128)(2,1)S(1)} %concatenate.3, s32[1024]{0:T(1024)S(1)} %pad_clamp_fusion.1), kind=kCustom, calls=%fused_computation | custom fusion | bytes 4196352 | tf_op jit(solution)/shard_map/gather | solution.py:26
  9.7 4.1 %reshape.77 = bf16[128,4,2048]{2,1,0:T(4,128)(2,1)} reshape(bf16[512,2048]{1,0:T(8,128)(2,1)} %gather_fusion) | data formatting | bytes 4194304 | tf_op jit(solution)/shard_map/reshape | solution.py:26
  13.8 42.4 %all_to_all.10 = bf16[128,4,2048]{2,1,0:T(4,128)(2,1)} all-to-all(bf16[128,4,2048]{2,1,0:T(4,128)(2,1)} %reshape.77), channel_id=1, replica_groups=mesh['ep'=32,'tp'=4] {'ep','tp'}, dimensions={0} | all-to-all | bytes 4194304 | tf_op jit(solution)/shard_map/all_to_all | solution.py:27
  56.2 4.0 %reshape.78 = bf16[512,2048]{1,0:T(8,128)(2,1)} reshape(bf16[128,4,2048]{2,1,0:T(4,128)(2,1)} %all_to_all.10) | data formatting | bytes 4194304 | tf_op jit(solution)/shard_map/reshape | solution.py:28
  60.1 4.4 %fusion.3 = f32[512,512]{1,0:T(8,128)} fusion(bf16[512,2048]{1,0:T(8,128)(2,1)} %reshape.78, bf16[1,2048,512]{2,1,0:T(8,128)(2,1)} %param.9), kind=kOutput, calls=%fused_computation.7 | convolution fusion | flops 1073741824 | bytes 5242880 | tf_op jit(solution)/shard_map/dot_general | solution.py:29
  64.6 0.0 copy-done
  64.6 6.2 %convolution_convert_fusion = bf16[512,2048]{1,0:T(8,128)(2,1)} fusion(bf16[1,512,2048]{2,1,0:T(8,128)(2,1)S(1)} %copy-done, bf16[512,2048]{1,0:T(8,128)(2,1)} %reshape.78, bf16[1,2048,512]{2,1,0:T(8,128)(2,1)} %param.10, f32[512,512]{1,0:T(8,128)} %fusion.3), kind=kOutput, calls=%fused_computation.3 | convolution fusion | flops 2150105088 | bytes 9437184 | tf_op jit(solution)/shard_map/dot_general | solution.py:32
  70.8 4.1 %reshape.79 = bf16[128,4,2048]{2,1,0:T(4,128)(2,1)} reshape(bf16[512,2048]{1,0:T(8,128)(2,1)} %convolution_convert_fusion) | data formatting | bytes 4194304 | tf_op jit(solution)/shard_map/reshape | solution.py:33
  74.9 0.0 copy-start.2
  74.9 5.0 %all-to-all-start.1 = ((bf16[128,4,2048]{2,1,0:T(4,128)(2,1)}), bf16[128,4,2048]{2,1,0:T(4,128)(2,1)}, u32[]{:S(2)}, u32[]{:S(2)}) async-start(bf16[128,4,2048]{2,1,0:T(4,128)(2,1)} %reshape.79), calls=%async_computation.1 | async-start | bytes 4194304 | tf_op jit(solution)/shard_map/all_to_all | solution.py:34
  79.9 0.0 copy-done.2
  80.0 0.1 copy.9
  80.1 30.4 %all-to-all-done.1 = bf16[128,4,2048]{2,1,0:T(4,128)(2,1)} async-done(((bf16[128,4,2048]{2,1,0:T(4,128)(2,1)}), bf16[128,4,2048]{2,1,0:T(4,128)(2,1)}, u32[]{:S(2)}, u32[]{:S(2)}) %all-to-all-start.1) | async-done | bytes 2097184 | tf_op jit(solution)/shard_map/all_to_all | solution.py:34
  110.4 4.0 %reshape.80 = bf16[512,2048]{1,0:T(8,128)(2,1)} reshape(bf16[128,4,2048]{2,1,0:T(4,128)(2,1)} %all-to-all-done.1) | data formatting | bytes 4194304 | tf_op jit(solution)/shard_map/reshape | solution.py:35
  114.4 4.2 %gather_fusion.1 = bf16[256,2048]{1,0:T(8,128)(2,1)S(1)} fusion(bf16[512,2048]{1,0:T(8,128)(2,1)} %reshape.80, s32[1024]{0:T(1024)S(1)} %pad_clamp_fusion), kind=kCustom, calls=%fused_computation.1 | custom fusion | bytes 2098176 | tf_op jit(solution)/shard_map/gather | solution.py:35
  118.6 2.4 %reshape.81 = f32[128,2,2048]{2,1,0:T(2,128)} reshape(bf16[256,2048]{1,0:T(8,128)(2,1)S(1)} %gather_fusion.1) | data formatting | bytes 3145728 | tf_op jit(solution)/shard_map/convert_element_type | solution.py:36
  121.0 5.6 %multiply_reduce_fusion = bf16[128,2048]{1,0:T(8,128)(2,1)} fusion(f32[128,2,2048]{2,1,0:T(2,128)} %reshape.81, f32[128,2]{1,0:T(8,128)S(1)} %copy.9), kind=kLoop, calls=%fused_computation.9 | loop fusion | flops 786432 | bytes 2622464 | tf_op jit(solution)/shard_map/reduce_sum | solution.py:37
  (14 shorter events, 0.2 us)
Async XLA Ops:
  0.0 64.6 %copy-start = (bf16[1,512,2048]{2,1,0:T(8,128)(2,1)S(1)}, bf16[1,512,2048]{2,1,0:T(8,128)(2,1)}, u32[]{:S(2)}) copy-start(bf16[1,512,2048]{2,1,0:T(8,128)(2,1)} %param.11) | copy-start | bytes 6291460
  0.0 5.5 %copy-start.1 = (bf16[128,2048]{1,0:T(8,128)(2,1)S(1)}, bf16[128,2048]{1,0:T(8,128)(2,1)}, u32[]{:S(2)}) copy-start(bf16[128,2048]{1,0:T(8,128)(2,1)} %param.7) | copy-start | bytes 1572868
  74.9 5.0 %copy-start.2 = (f32[128,2]{0,1:T(2,128)S(1)}, f32[128,2]{0,1:T(2,128)}, u32[]{:S(2)}) copy-start(f32[128,2]{0,1:T(2,128)} %param.13) | copy-start | bytes 3076
  74.9 35.5 %all-to-all-start.1 = ((bf16[128,4,2048]{2,1,0:T(4,128)(2,1)}), bf16[128,4,2048]{2,1,0:T(4,128)(2,1)}, u32[]{:S(2)}, u32[]{:S(2)}) async-start(bf16[128,4,2048]{2,1,0:T(4,128)(2,1)} %reshape.79), calls=%async_computation.1 | async-start | bytes 4194304 | tf_op jit(solution)/shard_map/all_to_all | solution.py:34
where the time goes:
time: 127 us
  blocking collectives  42.4 us (33%)
  waiting for transfers between devices  30.4 us (24%)
  local copies, waits for them, and re-layouts  29.2 us (23%)
  matrix products  10.7 us (8%)
  other arithmetic  8.86 us (7%)
  starting transfers between devices  5.02 us (4%)
    all_to_all x1, blocking collectives, local(): lax.all_to_all(outgoing, ('ep', 'tp'), split_axis=0, concat_axis=0, tiled...  42.4 us
    all_to_all x1, waiting for transfers between devices, local(): lax.all_to_all(answered, ('ep', 'tp'), split_axis=0, concat_axis=0, tiled...  30.4 us
    dot_general x1, matrix products, local(): jnp.dot(hidden, w_down[0], preferred_element_type=jnp.float32)  6.22 us
    reduce_sum x1, other arithmetic, local(): combined = jnp.sum(gate_weight[:, :, None] * picked, axis=1)  5.59 us
    all_to_all x1, starting transfers between devices, local(): lax.all_to_all(answered, ('ep', 'tp'), split_axis=0, concat_axis=0, tiled...  5.02 us
    dot_general x1, matrix products, local(): jnp.dot(slot_rows, w_gate[0], preferred_element_type=jnp.float32)  4.44 us
    gather x1, local copies, waits for them, and re-layouts, local(): picked = returned.reshape(experts * capacity, width)[position]  4.22 us
    reshape x1, local copies, waits for them, and re-layouts, local(): answered = expert_out.reshape(arrived.shape)  4.11 us
  transfers between devices with their start and end apart: 1, of which 1 were waited for; matrix products, arithmetic and copies ran while one was open for 0% of the time, Pallas kernels for 0%

commit v1 on v0

v1 whole, which is shorter than its diff:
```python
import functools

import jax
import jax.numpy as jnp
from jax import lax
from jax.experimental import pallas as pl
from jax.experimental.pallas import tpu as pltpu
from jax.sharding import PartitionSpec as P

MESH = pl.DeviceIdType.MESH
F32, BF16, I32 = jnp.float32, jnp.bfloat16, jnp.int32
HIGHEST = lax.Precision.HIGHEST

PAIRS = (
    (0, 0), (0, 1), (0, 3), (1, 0),
    (0, 2), (2, 0), (3, 1), (1, 2),
    (2, 2), (2, 1), (2, 3), (3, 2),
    (3, 0), (1, 1), (3, 3), (1, 3),
)
SLOTS = 32
CHUNKS = 4
PER = SLOTS // CHUNKS
HALF = PER // 2
CAP = 4
QUART = 4
BLOCK = CAP * QUART
AGA, AGB, FWD, RS1, RS2A, RS2B = range(6)
RIGHT, LEFT = 0, 1


def iota(shape, dim):
    return lax.broadcasted_iota(I32, shape, dim)


def onehot(mask):
    return jnp.where(mask, 1.0, 0.0).astype(BF16)


def kernel(tok_ref, gain_ref, wg_hbm, wu_hbm, wd_hbm, route_ref, gw_ref, out_ref,
           wg, wu, wd, stack, place, unplace, spread, gather, msgs, meta_out, xbuf, xmeta, mrows, gall,
           rows, ybuf, cbuf, rs1, rs2, back, ret,
           w_sem, y_send, y_recv, m_send, m_recv, x_send, x_recv, xm_send, xm_recv, b_send, b_recv):
    tokens, width = tok_ref.shape
    part = width // QUART
    me = lax.axis_index("ep")
    mx = lax.axis_index("tp")
    z, y, c = me // 8, (me // 2) % 4, me % 2
    right = {"tp": (mx + 1) % 4}
    left = {"tp": (mx + 3) % 4}

    def peer(slot, sign):
        dz, dy = PAIRS[slot // 2]
        dc = slot % 2
        return {"ep": ((z + 4 + sign * dz) % 4) * 8 + ((y + 4 + sign * dy) % 4) * 2 + (c + dc) % 2}

    weights = [pltpu.make_async_copy(src.at[0], dst, w_sem.at[n])
               for n, (src, dst) in enumerate(((wg_hbm, wg), (wu_hbm, wu), (wd_hbm, wd)))]
    for copy in weights:
        copy.start()

    barrier = pltpu.get_barrier_semaphore()
    for slot in range(1, SLOTS):
        pl.semaphore_signal(barrier, inc=1, device_id=peer(slot, -1), device_id_type=MESH)
    for side in (right, left):
        pl.semaphore_signal(barrier, inc=1, device_id=side, device_id_type=MESH)

    values = tok_ref[...].astype(F32)
    scale = lax.rsqrt(jnp.mean(values * values, axis=-1, keepdims=True) + 1e-06)
    normed = (values * scale * gain_ref[...]).astype(BF16)
    for q in range(QUART):
        stack[q * tokens:(q + 1) * tokens, :] = normed[:, q * part:(q + 1) * part]

    first = route_ref[:, 0:1]
    second = route_ref[:, 1:2]
    square = jnp.broadcast_to((first // 4).astype(F32), (tokens, tokens))
    turned = square.T
    same = square == turned
    row_id, col_id = iota((tokens, tokens), 0), iota((tokens, tokens), 1)
    rank_col = jnp.sum(jnp.where(same & (col_id < row_id), 1, 0), axis=1, keepdims=True)
    rank_row = jnp.sum(jnp.where(same & (row_id < col_id), 1, 0), axis=0, keepdims=True)

    def slot_of(group):
        rel = ((z + 4 - group // 8) % 4) * 4 + (y + 4 - (group // 2) % 4) % 4
        pair = jnp.zeros_like(group)
        for n, (dz, dy) in enumerate(PAIRS):
            pair = pair + jnp.where(rel == dz * 4 + dy, n, 0)
        return pair * 2 + (group + c) % 2

    slot_col = slot_of(first // 4)
    slot_row = slot_of(turned[0:1, :].astype(I32))
    pos_col = slot_col * CAP + rank_col
    pos_row = slot_row * CAP + rank_row

    r = iota((SLOTS * BLOCK, tokens), 0)
    place_of_r = (r // BLOCK) * CAP + r % CAP
    hit = place_of_r == pos_row
    for q in range(QUART):
        place[:, q * tokens:(q + 1) * tokens] = onehot(hit & ((r // CAP) % QUART == q))
    msgs[...] = jnp.dot(place[...], stack[...], preferred_element_type=F32).astype(BF16).reshape(SLOTS, BLOCK, part)
    xbuf[0, 0] = msgs[0]

    lane = iota((tokens, 128), 1)
    of_lane = (jnp.where(first % 4 == lane % 4, gw_ref[:, 0:1], 0.0)
               + jnp.where(second % 4 == lane % 4, gw_ref[:, 1:2], 0.0))
    of_lane = jnp.where(rank_col == lane // 4, of_lane, 0.0)
    chosen = jnp.where(iota((SLOTS, tokens), 0) == slot_row, 1.0, 0.0)
    meta = jnp.dot(chosen, of_lane, preferred_element_type=F32, precision=HIGHEST)
    for slot in range(SLOTS):
        meta_out[slot] = meta[slot:slot + 1, :]
    xmeta[0, 0] = meta[0:1, :]

    pl.semaphore_wait(barrier, SLOTS + 1)

    def remote(src, dst, send, recv, device):
        return pltpu.make_async_remote_copy(src_ref=src, dst_ref=dst, send_sem=send, recv_sem=recv,
                                            device_id=device, device_id_type=MESH)

    for slot in range(1, SLOTS):
        remote(msgs.at[slot], xbuf.at[0, slot], y_send.at[slot // PER], y_recv.at[slot // PER], peer(slot, -1)).start()
        if slot == PER - 1:
            for other in range(1, SLOTS):
                remote(meta_out.at[other], xmeta.at[0, other], m_send, m_recv, peer(other, -1)).start()

    half = 2 * PER * BLOCK
    a, b = iota((half, half), 0), iota((half, half), 1)
    piece = PER * BLOCK
    run = PER * CAP

    def other_order(n):
        return (n // piece) * piece + ((n % run) // CAP) * BLOCK + ((n % piece) // run) * CAP + n % CAP
    spread[...] = onehot(other_order(a) == b)
    gather[...] = onehot(other_order(b) == a)
    r = iota((tokens, SLOTS * BLOCK), 1)
    hit = (r // BLOCK) * CAP + r % CAP == pos_col
    for q in range(QUART):
        unplace[q * tokens:(q + 1) * tokens, :] = onehot(hit & ((r // CAP) % QUART == q))

    def lo(j):
        return slice(j * PER, j * PER + HALF)

    def hi(j):
        return slice(j * PER + HALF, (j + 1) * PER)

    def both(j):
        return slice(j * PER, (j + 1) * PER)

    def ag(side, kind, j):
        part_of = lo(j) if kind == AGA else hi(j)
        to = 1 if side == RIGHT else 3
        return remote(xbuf.at[0, part_of], xbuf.at[to, part_of], x_send.at[side, kind, j], x_recv.at[side, kind, j],
                      right if side == RIGHT else left)

    def fwd(side, j):
        part_of, held = (lo(j), 1) if side == RIGHT else (hi(j), 3)
        return remote(xbuf.at[held, part_of], xbuf.at[2, part_of], x_send.at[side, FWD, j], x_recv.at[side, FWD, j],
                      right if side == RIGHT else left)

    def rs_first(side, j):
        part_of = lo(j) if side == RIGHT else hi(j)
        return remote(cbuf.at[2, part_of], rs1.at[side, j], x_send.at[side, RS1, j], x_recv.at[side, RS1, j],
                      right if side == RIGHT else left)

    def rs_second(side, kind, j):
        part_of = lo(j) if kind == RS2A else hi(j)
        held = 3 if side == RIGHT else 1
        return remote(cbuf.at[held, part_of], rs2.at[side, part_of], x_send.at[side, kind, j], x_recv.at[side, kind, j],
                      right if side == RIGHT else left)

    def start_gather(j):
        src = xbuf.at[0, slice(j * PER + (1 if j == 0 else 0), (j + 1) * PER)]
        remote(src, src, y_send.at[j], y_recv.at[j], right).wait_recv()
        ag(RIGHT, AGA, j).start()
        ag(LEFT, AGB, j).start()
        ag(RIGHT, AGB, j).start()
        ag(LEFT, AGA, j).start()

    def forward(j):
        ag(RIGHT, AGA, j).wait_recv()
        fwd(RIGHT, j).start()
        ag(LEFT, AGB, j).wait_recv()
        fwd(LEFT, j).start()

    def meta_gather():
        src = xmeta.at[0, slice(1, SLOTS)]
        remote(src, src, m_send, m_recv, right).wait_recv()
        remote(xmeta.at[0], xmeta.at[1], xm_send.at[0], xm_recv.at[0], right).start()
        remote(xmeta.at[0], xmeta.at[3], xm_send.at[1], xm_recv.at[1], left).start()

    def meta_forward():
        remote(xmeta.at[0], xmeta.at[1], xm_send.at[0], xm_recv.at[0], right).wait_recv()
        remote(xmeta.at[1], xmeta.at[2], xm_send.at[2], xm_recv.at[2], right).start()
        remote(xmeta.at[0], xmeta.at[3], xm_send.at[1], xm_recv.at[1], left).wait_recv()

    def meta_use():
        remote(xmeta.at[1], xmeta.at[2], xm_send.at[2], xm_recv.at[2], right).wait_recv()
        for side in range(4):
            for slot in range(SLOTS):
                mrows[side * SLOTS + slot:side * SLOTS + slot + 1, :] = xmeta[side, slot]
        n = iota((CHUNKS * 4 * run, 4 * SLOTS), 0)
        col = iota((CHUNKS * 4 * run, 4 * SLOTS), 1)
        source = ((n // run) % 4) * SLOTS + (n // (4 * run)) * PER + (n % run) // CAP
        picked = jnp.dot(jnp.where(source == col, 1.0, 0.0), mrows[...], preferred_element_type=F32, precision=HIGHEST)
        mine = (n % CAP) * 4 + mx == col
        gall[...] = jnp.broadcast_to(jnp.sum(jnp.where(mine, picked, 0.0), axis=1, keepdims=True), gall.shape)

    def compute(j):
        ag(RIGHT, AGB, j).wait_recv()
        ag(LEFT, AGA, j).wait_recv()
        fwd(RIGHT, j).wait_recv()
        fwd(LEFT, j).wait_recv()
        for pair in range(2):
            block = xbuf[2 * pair:2 * pair + 2, both(j)].reshape(half, part)
            ordered = jnp.dot(spread[...], block, preferred_element_type=F32).astype(BF16)
            for side in range(2):
                for q in range(QUART):
                    at = (2 * pair + side) * run
                    rows[at:at + run, q * part:(q + 1) * part] = ordered[side * piece + q * run:side * piece + (q + 1) * run]
        if j == 0:
            weights[0].wait()
            weights[1].wait()
        gate = jnp.dot(rows[...], wg[...], preferred_element_type=F32)
        up = jnp.dot(rows[...], wu[...], preferred_element_type=F32)
        hidden = (gate / (1.0 + jnp.exp(-gate)) * up).astype(BF16)
        if j == 0:
            weights[2].wait()
            meta_use()
        weight = gall[j * 4 * run:(j + 1) * 4 * run, 0:1]
        for q in range(QUART):
            piece_out = jnp.dot(hidden, wd[:, q * part:(q + 1) * part], preferred_element_type=F32)
            piece_out = (piece_out * weight).astype(BF16)
            for side in range(4):
                ybuf[side * piece + q * run:side * piece + (q + 1) * run, :] = piece_out[side * run:(side + 1) * run]
        for pair in (1, 0):
            block = jnp.dot(gather[...], ybuf[pair * half:(pair + 1) * half, :], preferred_element_type=F32).astype(BF16)
            cbuf[2 * pair:2 * pair + 2, both(j)] = block.reshape(2, PER, BLOCK, part)
            if pair == 1:
                rs_first(RIGHT, j).start()
                rs_first(LEFT, j).start()
        rs_second(RIGHT, RS2B, j).start()
        rs_second(LEFT, RS2A, j).start()

    def reduce_first(j):
        rs_first(RIGHT, j).wait_recv()
        cbuf[3, lo(j)] = (cbuf[3, lo(j)].astype(F32) + rs1[RIGHT, j].astype(F32)).astype(BF16)
        rs_second(RIGHT, RS2A, j).start()
        rs_first(LEFT, j).wait_recv()
        cbuf[1, hi(j)] = (cbuf[1, hi(j)].astype(F32) + rs1[LEFT, j].astype(F32)).astype(BF16)
        rs_second(LEFT, RS2B, j).start()

    def give_back(j):
        for side in (RIGHT, LEFT):
            rs_second(side, RS2A, j).wait_recv()
            rs_second(side, RS2B, j).wait_recv()
        total = cbuf[0, both(j)].astype(F32) + rs2[RIGHT, both(j)].astype(F32) + rs2[LEFT, both(j)].astype(F32)
        back[both(j)] = total.astype(BF16)
        if j == 0:
            ret[0] = back[0]
        for slot in range(max(1, j * PER), (j + 1) * PER):
            remote(back.at[slot], ret.at[slot], b_send.at[j], b_recv.at[j], peer(slot, 1)).start()

    start_gather(0)
    start_gather(1)
    forward(0)
    meta_gather()
    start_gather(2)
    forward(1)
    meta_forward()
    compute(0)
    start_gather(3)
    forward(2)
    compute(1)
    reduce_first(0)
    forward(3)
    compute(2)
    reduce_first(1)
    give_back(0)
    compute(3)
    reduce_first(2)
    give_back(1)
    reduce_first(3)
    give_back(2)
    give_back(3)

    for j in range(CHUNKS):
        src = ret.at[slice(j * PER + (1 if j == 0 else 0), (j + 1) * PER)]
        remote(src, src, b_send.at[j], b_recv.at[j], right).wait_recv()
    result = jnp.dot(unplace[...], ret[...].reshape(SLOTS * BLOCK, part), preferred_element_type=F32).astype(BF16)
    for q in range(QUART):
        out_ref[:, q * part:(q + 1) * part] = result[q * tokens:(q + 1) * tokens]

    for j in range(CHUNKS):
        src = msgs.at[slice(j * PER + (1 if j == 0 else 0), (j + 1) * PER)]
        remote(src, src, y_send.at[j], y_recv.at[j], right).wait_send()
        remote(src, src, b_send.at[j], b_recv.at[j], right).wait_send()
        for side in (RIGHT, LEFT):
            ag(side, AGA, j).wait_send()
            ag(side, AGB, j).wait_send()
            fwd(side, j).wait_send()
            rs_first(side, j).wait_send()
            rs_second(side, RS2A, j).wait_send()
            rs_second(side, RS2B, j).wait_send()
    src = meta_out.at[slice(1, SLOTS)]
    remote(src, src, m_send, m_recv, right).wait_send()
    for n in range(3):
        remote(xmeta.at[0], xmeta.at[1], xm_send.at[n], xm_recv.at[n], right).wait_send()


def local(tokens, norm_gain, w_gate, w_up, w_down, routing, gate_weight):
    count, width = tokens.shape
    hidden = w_gate.shape[2]
    part = width // QUART
    total = SLOTS * BLOCK
    vmem = pl.BlockSpec(memory_space=pltpu.VMEM)
    hbm = pl.BlockSpec(memory_space=pltpu.HBM)
    dma = pltpu.SemaphoreType.DMA
    return pl.pallas_call(
        kernel,
        out_shape=jax.ShapeDtypeStruct((count, width), BF16),
        in_specs=[vmem, vmem, hbm, hbm, hbm, vmem, vmem],
        out_specs=vmem,
        scratch_shapes=[
            pltpu.VMEM((width, hidden), BF16),
            pltpu.VMEM((width, hidden), BF16),
            pltpu.VMEM((hidden, width), BF16),
            pltpu.VMEM((QUART * count, part), BF16),
            pltpu.VMEM((total, QUART * count), BF16),
            pltpu.VMEM((QUART * count, total), BF16),
            pltpu.VMEM((2 * PER * BLOCK, 2 * PER * BLOCK), BF16),
            pltpu.VMEM((2 * PER * BLOCK, 2 * PER * BLOCK), BF16),
            pltpu.VMEM((SLOTS, BLOCK, part), BF16),
            pltpu.VMEM((SLOTS, 1, 128), F32),
            pltpu.VMEM((4, SLOTS, BLOCK, part), BF16),
            pltpu.VMEM((4, SLOTS, 1, 128), F32),
            pltpu.VMEM((4 * SLOTS, 128), F32),
            pltpu.VMEM((4 * SLOTS * CAP, 128), F32),
            pltpu.VMEM((4 * PER * CAP, width), BF16),
            pltpu.VMEM((4 * PER * BLOCK, part), BF16),
            pltpu.VMEM((4, SLOTS, BLOCK, part), BF16),
            pltpu.VMEM((2, CHUNKS, HALF, BLOCK, part), BF16),
            pltpu.VMEM((2, SLOTS, BLOCK, part), BF16),
            pltpu.VMEM((SLOTS, BLOCK, part), BF16),
            pltpu.VMEM((SLOTS, BLOCK, part), BF16),
            dma((3,)), dma((CHUNKS,)), dma((CHUNKS,)), dma, dma,
            dma((2, 6, CHUNKS)), dma((2, 6, CHUNKS)), dma((3,)), dma((3,)), dma((CHUNKS,)), dma((CHUNKS,)),
        ],
        compiler_params=pltpu.CompilerParams(
            collective_id=0, has_side_effects=True, vmem_limit_bytes=56 * 1024 * 1024
        ),
    )(tokens, norm_gain.reshape(1, width), w_gate, w_up, w_down, routing, gate_weight)


def solution(mesh):
    placed = (
        P(("ep", "tp"), None),
        P(),
        P(("ep", "tp"), None, None),
        P(("ep", "tp"), None, None),
        P(("ep", "tp"), None, None),
        P(("ep", "tp"), None),
        P(("ep", "tp"), None),
    )
    return jax.shard_map(
        local, mesh=mesh, in_specs=placed, out_specs=P(("ep", "tp"), None), check_vma=False
    )
```

time: 127 us -> 66.3 us (0.52)
  Pallas kernels: 0 us -> 61.4 us
  blocking collectives: 42.4 us -> 0 us
  waiting for transfers between devices: 30.4 us -> 0 us
  local copies, waits for them, and re-layouts: 29.2 us -> 4.7 us
  matrix products: 10.7 us -> 0 us
  other arithmetic: 8.86 us -> 0 us
  starting transfers between devices: 5.02 us -> 0 us
    pallas_call x0 -> x1, Pallas kernels: none -> 61.4 us  [local(): pl.pallas_call(kernel, out_shape=jax.ShapeDtypeStruct((count, width), BF1...]
    all_to_all x1 -> x0, blocking collectives: 42.4 us -> none  [local(): lax.all_to_all(outgoing, ('ep', 'tp'), split_axis=0, concat_axis=0, tiled...]
    all_to_all x1 -> x0, waiting for transfers between devices: 30.4 us -> none  [local(): lax.all_to_all(answered, ('ep', 'tp'), split_axis=0, concat_axis=0, tiled...]
    reshape x4 -> x0, local copies, waits for them, and re-layouts: 16.1 us -> none  [the longest x1 4.11 us: local(): answered = expert_out.reshape(arrived.shape)]
    dot_general x2 -> x0, matrix products: 10.7 us -> none  [the longest x1 6.22 us: local(): jnp.dot(hidden, w_down[0], preferred_element_type=jnp.float32)]
    gather x2 -> x0, local copies, waits for them, and re-layouts: 7.52 us -> none  [the longest x1 4.22 us: local(): picked = returned.reshape(experts * capacity, width)[position]]
    reduce_sum x3 -> x0, other arithmetic: 6.99 us -> none  [the longest x1 5.59 us: local(): combined = jnp.sum(gate_weight[:, :, None] * picked, axis=1)]
    all_to_all x1 -> x0, starting transfers between devices: 5.02 us -> none  [local(): lax.all_to_all(answered, ('ep', 'tp'), split_axis=0, concat_axis=0, tiled...]
  transfers between devices with their start and end apart: 1 -> 0, of which waited for: 1 -> 0; matrix products, arithmetic and copies ran while one was open for 0% -> 0% of each run, Pallas kernels for 0% -> 0%
where the time goes in v1:
time: 66.3 us; the launch traced here: 66.1 us
  Pallas kernels  61.4 us (93%)
  local copies, waits for them, and re-layouts  4.7 us (7%)
    pallas_call x1, Pallas kernels, local(): pl.pallas_call(kernel, out_shape=jax.ShapeDtypeStruct((count, width), BF1...  61.4 us
    unnamed x3, local copies, waits for them, and re-layouts  4.7 us

profile of v1, /device:TPU:1, one launch (start us, length us, event | category | flops | bytes accessed | tf_op | source)
XLA Modules:
  0.0 66.1 jit_solution(17339955596258525431)
XLA Ops:
  0.0 1.4 %copy.8.route_ref = s32[128,2]{1,0:T(8,128)} copy(s32[128,2]{0,1:T(2,128)} %param.12) | data formatting | bytes 2048 | tf_op args[5]
  1.4 1.4 %copy.9.gw_ref = f32[128,2]{1,0:T(8,128)} copy(f32[128,2]{0,1:T(2,128)} %param.13) | data formatting | bytes 2048 | tf_op args[6]
  2.8 61.4 %shard_map.73 = bf16[128,2048]{1,0:T(8,128)(2,1)} custom-call(bf16[128,2048]{1,0:T(8,128)(2,1)} %tok_ref.1, f32[1,2048]{1,0:T(1,128)} %bitcast.1, bf16[1,2048,512]{2,1,0:T(8,128)(2,1)} %wg_hbm.1, bf16[1,2048,512]{2,1,0:T(8,128)(2,1)} %wu_hbm.1, bf16[1,512,2048]{2,1,0:T(8,128)(2,1)} %wd_hbm.1, s32[128,2]{1,0:T(8,128)} %copy.8.route_ref, f32[128,2]{1,0:T(8,128)} %copy.9.gw_ref), custom_call_target="tpu_custom_call" | custom-call | tf_op jit(solution)/shard_map/pallas_call | solution.py:316
  64.2 1.9 %copy.11 = bf16[128,2048]{1,0:T(8,128)(2,1)} copy(bf16[128,2048]{1,0:T(8,128)(2,1)} %shard_map.73) | data formatting | bytes 1048576

commit v2 on v0

v2 whole, which is shorter than its diff:
```python
import functools

import jax
import jax.numpy as jnp
from jax import lax
from jax.experimental import pallas as pl
from jax.experimental.pallas import tpu as pltpu
from jax.sharding import PartitionSpec as P

MESH = pl.DeviceIdType.MESH
F32, BF16, I32 = jnp.float32, jnp.bfloat16, jnp.int32
HIGHEST = lax.Precision.HIGHEST

CHUNKS = {
    "E": ((0, 0),),
    "A": ((0, 1), (0, 3), (1, 0), (3, 0)),
    "B": ((2, 0), (2, 1), (0, 2), (1, 2)),
    "D": ((1, 1), (3, 3), (1, 3)),
    "C": ((2, 2), (2, 3), (3, 2), (3, 1)),
}
NAMES = tuple(CHUNKS)
DIRECT = "EA"
PAIRS = tuple(pair for name in NAMES for pair in CHUNKS[name])
SLOTS = 2 * len(PAIRS)
COUNT = {name: 2 * len(CHUNKS[name]) for name in NAMES}
START = {name: 2 * PAIRS.index(CHUNKS[name][0]) for name in NAMES}
CAP = 4
QUART = 4
BLOCK = CAP * QUART
AGA, AGB, FWD, RS1, RS2A, RS2B = range(6)
RIGHT, LEFT = 0, 1
SIZES = tuple(sorted(set(COUNT.values())))
ORDER = (
    "dE", "oD", "dA", "oB", "oC", "k", "fE", "gD", "fA", "mS", "gB", "fD", "gC", "fB", "mU", "fC",
    "cD", "cB", "cC", "rB", "rC", "cA", "rD", "cE", "bB", "bC", "rA", "bD", "rE", "bA", "bE",
)


def iota(shape, dim):
    return lax.broadcasted_iota(I32, shape, dim)


def onehot(mask):
    return jnp.where(mask, 1.0, 0.0).astype(BF16)


def kernel(tok_hbm, gain_hbm, wg_hbm, wu_hbm, wd_hbm, route_hbm, gw_hbm, out_ref,
           tok_ref, gain_ref, route_ref, gw_ref, wg, wu, wd, stack, place, unplace, spreads, gathers, msgs, meta_out, xbuf, xmeta, mrows, gall,
           rows, ybuf, cbuf, rs1, rs2, back, ret,
           w_sem, y_send, y_recv, m_send, m_recv, x_send, x_recv, xm_send, xm_recv, b_send, b_recv):
    tokens, width = tok_ref.shape
    part = width // QUART
    me = lax.axis_index("ep")
    mx = lax.axis_index("tp")
    z, y, c = me // 8, (me // 2) % 4, me % 2
    right = {"tp": (mx + 1) % 4}
    left = {"tp": (mx + 3) % 4}

    def peer(slot, sign, dx=0):
        dz, dy = PAIRS[slot // 2]
        dc = slot % 2
        group = ((z + 4 + sign * dz) % 4) * 8 + ((y + 4 + sign * dy) % 4) * 2 + (c + dc) % 2
        return {"ep": group, "tp": (mx + 4 + dx) % 4}

    def slots_of(name):
        return range(START[name], START[name] + COUNT[name])

    small = [pltpu.make_async_copy(src, dst, w_sem.at[3 + n]) for n, (src, dst) in enumerate((
        (tok_hbm, tok_ref), (gain_hbm, gain_ref), (route_hbm, route_ref), (gw_hbm, gw_ref)))]
    for copy in small:
        copy.start()
    weights = [pltpu.make_async_copy(src.at[0], dst, w_sem.at[n])
               for n, (src, dst) in enumerate(((wg_hbm, wg), (wu_hbm, wu), (wd_hbm, wd)))]

    barrier = pltpu.get_barrier_semaphore()
    for slot in range(1, SLOTS):
        pl.semaphore_signal(barrier, inc=1, device_id=peer(slot, -1), device_id_type=MESH)
    near = [slot for name in DIRECT for slot in slots_of(name) if slot]
    for slot in near:
        for dx in (1, -1):
            pl.semaphore_signal(barrier, inc=1, device_id=peer(slot, -1, dx), device_id_type=MESH)
    for side in (right, {"tp": (mx + 2) % 4}, left):
        pl.semaphore_signal(barrier, inc=1, device_id=side, device_id_type=MESH)

    for copy in small:
        copy.wait()
    for copy in weights:
        copy.start()
    values = tok_ref[...].astype(F32)
    scale = lax.rsqrt(jnp.mean(values * values, axis=-1, keepdims=True) + 1e-06)
    normed = (values * scale * gain_ref[...]).astype(BF16)
    for q in range(QUART):
        stack[q * tokens:(q + 1) * tokens, :] = normed[:, q * part:(q + 1) * part]

    first = route_ref[0:1, :]
    second = route_ref[1:2, :]
    group = first // 4
    square = jnp.broadcast_to(group.astype(F32), (tokens, tokens))
    earlier = (square.T == square) & (iota((tokens, tokens), 0) < iota((tokens, tokens), 1))
    rank = jnp.sum(jnp.where(earlier, 1, 0), axis=0, keepdims=True)

    def slot_of(group):
        rel = ((z + 4 - group // 8) % 4) * 4 + (y + 4 - (group // 2) % 4) % 4
        pair = jnp.zeros_like(group)
        for n, (dz, dy) in enumerate(PAIRS):
            pair = pair + jnp.where(rel == dz * 4 + dy, n, 0)
        return pair * 2 + (group + c) % 2

    slot_row = slot_of(group)
    pos_row = slot_row * CAP + rank
    pos_col = jnp.broadcast_to(pos_row.astype(F32), (tokens, tokens)).T[:, 0:1].astype(I32)

    r = iota((SLOTS * BLOCK, tokens), 0)
    place_of_r = (r // BLOCK) * CAP + r % CAP
    hit = place_of_r == pos_row
    for q in range(QUART):
        place[:, q * tokens:(q + 1) * tokens] = onehot(hit & ((r // CAP) % QUART == q))
    msgs[...] = jnp.dot(place[...], stack[...], preferred_element_type=F32).astype(BF16).reshape(SLOTS, BLOCK, part)
    xbuf[0, 0] = msgs[0]

    line = iota((128, tokens), 0)
    of_line = (jnp.where(first % 4 == line % 4, gw_ref[0:1, :], 0.0)
               + jnp.where(second % 4 == line % 4, gw_ref[1:2, :], 0.0))
    of_line = jnp.where(rank == line // 4, of_line, 0.0)
    chosen = jnp.where(iota((SLOTS, tokens), 0) == slot_row, 1.0, 0.0)
    meta = lax.dot_general(chosen, of_line, (((1,), (1,)), ((), ())), preferred_element_type=F32, precision=HIGHEST)
    for slot in range(SLOTS):
        meta_out[0, slot] = meta[slot:slot + 1, :]

    with jax.named_scope("barrier"):
        pl.semaphore_wait(barrier, SLOTS + 2 + 2 * len(near))

    def remote(src, dst, send, recv, device):
        return pltpu.make_async_remote_copy(src_ref=src, dst_ref=dst, send_sem=send, recv_sem=recv,
                                            device_id=device, device_id_type=MESH)

    sides = (right, {"tp": (mx + 2) % 4}, left)
    for n, side in enumerate(sides):
        remote(meta_out.at[0], meta_out.at[n + 1], xm_send.at[n], xm_recv.at[n], side).start()

    def span(name, kind):
        first_slot, count = START[name], COUNT[name]
        low, high = {None: (0, count), AGA: (0, count // 2), AGB: (count // 2, count)}[kind]
        return slice(first_slot + low, first_slot + high)

    def send_over(name):
        for slot in slots_of(name):
            if slot:
                n = NAMES.index(name)
                remote(msgs.at[slot], xbuf.at[0, slot], y_send, y_recv.at[n], peer(slot, -1)).start()

    def send_direct(name):
        n = NAMES.index(name)
        at, count = START[name], COUNT[name]
        for step in range(count):
            for side, held, slot in ((RIGHT, 1, at + step), (LEFT, 3, at + (step + count // 2) % count)):
                kind = AGA if slot < at + count // 2 else AGB
                remote(msgs.at[slot], xbuf.at[held, slot], x_send.at[side], x_recv.at[side, kind, n],
                       peer(slot, -1, -1 if side else 1)).start()
        send_over(name)

    def constants():
        for size, spread, gather in zip(SIZES, spreads, gathers):
            edge = 2 * size * BLOCK
            run = 2 * size * CAP
            a, b = iota((edge, edge), 0), iota((edge, edge), 1)
            spread[...] = onehot(((a % run) // CAP) * BLOCK + (a // run) * CAP + a % CAP == b)
            gather[...] = onehot(((b % run) // CAP) * BLOCK + (b // run) * CAP + b % CAP == a)
        r = iota((tokens, SLOTS * BLOCK), 1)
        hit = (r // BLOCK) * CAP + r % CAP == pos_col
        for q in range(QUART):
            unplace[q * tokens:(q + 1) * tokens, :] = onehot(hit & ((r // CAP) % QUART == q))

    def hop(side, src, dst, kind, name):
        return remote(src, dst, x_send.at[side], x_recv.at[side, kind, NAMES.index(name)], left if side else right)

    def ag(side, kind, name):
        part_of = span(name, kind)
        return hop(side, xbuf.at[0, part_of], xbuf.at[3 if side else 1, part_of], kind, name)

    def fwd(side, name):
        part_of = span(name, side)
        return hop(side, xbuf.at[3 if side else 1, part_of], xbuf.at[2, part_of], FWD, name)

    def rs_first(side, name):
        part_of = span(name, side)
        return hop(side, cbuf.at[2, part_of], rs1.at[part_of], RS1, name)

    def rs_second(side, kind, name):
        part_of = span(name, kind - RS2A)
        return hop(side, cbuf.at[1 if side else 3, part_of], rs2.at[side, part_of], kind, name)

    def over_done(name):
        first_slot = max(1, START[name])
        src = xbuf.at[0, slice(first_slot, START[name] + COUNT[name])]
        remote(src, src, y_send, y_recv.at[NAMES.index(name)], right).wait_recv()

    def start_gather(name):
        over_done(name)
        ag(RIGHT, AGA, name).start()
        ag(LEFT, AGB, name).start()
        ag(RIGHT, AGB, name).start()
        ag(LEFT, AGA, name).start()

    def forward(name):
        ag(RIGHT, AGA, name).wait_recv()
        fwd(RIGHT, name).start()
        ag(LEFT, AGB, name).wait_recv()
        fwd(LEFT, name).start()

    def meta_send():
        for n, side in enumerate(sides):
            remote(meta_out.at[0], meta_out.at[n + 1], xm_send.at[n], xm_recv.at[n], side).wait_recv()
        for slot in range(1, SLOTS):
            remote(meta_out.at[:, slot], xmeta.at[:, slot], m_send, m_recv, peer(slot, -1)).start()

    def meta_use():
        src = xmeta.at[:, slice(1, SLOTS)]
        remote(src, src, m_send, m_recv, right).wait_recv()
        for side in range(4):
            for slot in range(SLOTS):
                row = xmeta[side, slot] if slot else meta_out[side, 0]
                mrows[side * SLOTS + slot:side * SLOTS + slot + 1, :] = row
        for name in NAMES:
            at, count = START[name], COUNT[name]
            n, col = iota((count * BLOCK, 4 * SLOTS), 0), iota((count * BLOCK, 4 * SLOTS), 1)
            source = (n // (count * CAP)) * SLOTS + at + (n % (count * CAP)) // CAP
            picked = jnp.dot(jnp.where(source == col, 1.0, 0.0), mrows[...], preferred_element_type=F32, precision=HIGHEST)
            mine = (n % CAP) * 4 + mx == col
            gall[at * BLOCK:(at + count) * BLOCK, :] = jnp.broadcast_to(
                jnp.sum(jnp.where(mine, picked, 0.0), axis=1, keepdims=True), (count * BLOCK, 128))

    started = []

    def compute(name):
        at, count = START[name], COUNT[name]
        spread, gather = spreads[SIZES.index(count)], gathers[SIZES.index(count)]
        edge, run, total_rows = 2 * count * BLOCK, 2 * count * CAP, 4 * count * CAP
        if name in DIRECT:
            over_done(name)
        ag(RIGHT, AGB, name).wait_recv()
        ag(LEFT, AGA, name).wait_recv()
        fwd(RIGHT, name).wait_recv()
        fwd(LEFT, name).wait_recv()
        for pair in range(2):
            block = xbuf[2 * pair:2 * pair + 2, span(name, None)].reshape(edge, part)
            ordered = jnp.dot(spread[...], block, preferred_element_type=F32).astype(BF16)
            for q in range(QUART):
                rows[pair * run:(pair + 1) * run, q * part:(q + 1) * part] = ordered[q * run:(q + 1) * run]
        if not started:
            weights[0].wait()
            weights[1].wait()
        inputs = rows[0:total_rows, :]
        gate = jnp.dot(inputs, wg[...], preferred_element_type=F32)
        up = jnp.dot(inputs, wu[...], preferred_element_type=F32)
        hidden = (gate / (1.0 + jnp.exp(-gate)) * up).astype(BF16)
        if not started:
            weights[2].wait()
            started.append(name)
        weight = gall[at * BLOCK:(at + count) * BLOCK, 0:1]
        for q in range(QUART):
            piece_out = jnp.dot(hidden, wd[:, q * part:(q + 1) * part], preferred_element_type=F32)
            piece_out = (piece_out * weight).astype(BF16)
            for pair in range(2):
                ybuf[pair * edge + q * run:pair * edge + (q + 1) * run, :] = piece_out[pair * run:(pair + 1) * run]
        for pair in (1, 0):
            block = jnp.dot(gather[...], ybuf[pair * edge:(pair + 1) * edge, :], preferred_element_type=F32).astype(BF16)
            cbuf[2 * pair:2 * pair + 2, span(name, None)] = block.reshape(2, count, BLOCK, part)
            if pair == 1:
                rs_first(RIGHT, name).start()
                rs_first(LEFT, name).start()
        rs_second(RIGHT, RS2B, name).start()
        rs_second(LEFT, RS2A, name).start()

    def reduce_first(name):
        for side, held, kind in ((RIGHT, 3, RS2A), (LEFT, 1, RS2B)):
            rs_first(side, name).wait_recv()
            mine = span(name, side)
            cbuf[held, mine] = (cbuf[held, mine].astype(F32) + rs1[mine].astype(F32)).astype(BF16)
            rs_second(side, kind, name).start()

    def give_back(name):
        for side in (RIGHT, LEFT):
            rs_second(side, RS2A, name).wait_recv()
            rs_second(side, RS2B, name).wait_recv()
        all_of = span(name, None)
        total = cbuf[0, all_of].astype(F32) + rs2[RIGHT, all_of].astype(F32) + rs2[LEFT, all_of].astype(F32)
        back[all_of] = total.astype(BF16)
        for slot in slots_of(name):
            if slot:
                remote(back.at[slot], ret.at[slot], b_send, b_recv, peer(slot, 1)).start()
            else:
                ret[0] = back[0]

    steps = {"d": send_direct, "g": start_gather, "f": forward, "c": compute, "r": reduce_first, "b": give_back, "o": send_over}
    plain = {"k": constants, "mS": meta_send, "mU": meta_use}
    for what in ORDER:
        with jax.named_scope(what):
            plain[what]() if what in plain else steps[what[0]](what[1])

    with jax.named_scope("sent"):
        src = msgs.at[slice(1, SLOTS)]
        remote(src, src, y_send, y_recv.at[0], right).wait_send()
        for side in (RIGHT, LEFT):
            src = xbuf.at[slice(0, 3)]
            remote(src, src, x_send.at[side], x_recv.at[0, 0, 0], right).wait_send()
        src = meta_out.at[:, slice(1, SLOTS)]
        remote(src, src, m_send, m_recv, right).wait_send()
        for n in range(3):
            remote(meta_out.at[0], meta_out.at[1], xm_send.at[n], xm_recv.at[n], right).wait_send()
    with jax.named_scope("back"):
        src = ret.at[slice(1, SLOTS)]
        remote(src, src, b_send, b_recv, right).wait_recv()
    with jax.named_scope("final"):
        result = jnp.dot(unplace[...], ret[...].reshape(SLOTS * BLOCK, part), preferred_element_type=F32).astype(BF16)
        for q in range(QUART):
            out_ref[:, q * part:(q + 1) * part] = result[q * tokens:(q + 1) * tokens]
        remote(src, src, b_send, b_recv, right).wait_send()


def local(tokens, norm_gain, w_gate, w_up, w_down, routing, gate_weight):
    count, width = tokens.shape
    hidden = w_gate.shape[2]
    part = width // QUART
    total = SLOTS * BLOCK
    vmem = pl.BlockSpec(memory_space=pltpu.VMEM)
    hbm = pl.BlockSpec(memory_space=pltpu.HBM)
    dma = pltpu.SemaphoreType.DMA
    return pl.pallas_call(
        kernel,
        out_shape=jax.ShapeDtypeStruct((count, width), BF16),
        in_specs=[hbm] * 7,
        out_specs=vmem,
        scratch_shapes=[
            pltpu.VMEM((count, width), BF16),
            pltpu.VMEM((1, width), F32),
            pltpu.VMEM((2, count), I32),
            pltpu.VMEM((2, count), F32),
            pltpu.VMEM((width, hidden), BF16),
            pltpu.VMEM((width, hidden), BF16),
            pltpu.VMEM((hidden, width), BF16),
            pltpu.VMEM((QUART * count, part), BF16),
            pltpu.VMEM((total, QUART * count), BF16),
            pltpu.VMEM((QUART * count, total), BF16),
            [pltpu.VMEM((2 * size * BLOCK, 2 * size * BLOCK), BF16) for size in SIZES],
            [pltpu.VMEM((2 * size * BLOCK, 2 * size * BLOCK), BF16) for size in SIZES],
            pltpu.VMEM((SLOTS, BLOCK, part), BF16),
            pltpu.VMEM((4, SLOTS, 1, 128), F32),
            pltpu.VMEM((4, SLOTS, BLOCK, part), BF16),
            pltpu.VMEM((4, SLOTS, 1, 128), F32),
            pltpu.VMEM((4 * SLOTS, 128), F32),
            pltpu.VMEM((4 * SLOTS * CAP, 128), F32),
            pltpu.VMEM((max(SIZES) * BLOCK, width), BF16),
            pltpu.VMEM((4 * max(SIZES) * BLOCK, part), BF16),
            pltpu.VMEM((4, SLOTS, BLOCK, part), BF16),
            pltpu.VMEM((SLOTS, BLOCK, part), BF16),
            pltpu.VMEM((2, SLOTS, BLOCK, part), BF16),
            pltpu.VMEM((SLOTS, BLOCK, part), BF16),
            pltpu.VMEM((SLOTS, BLOCK, part), BF16),
            dma((7,)), dma, dma((len(NAMES),)), dma, dma,
            dma((2,)), dma((2, 6, len(NAMES))), dma((3,)), dma((3,)), dma, dma,
        ],
        compiler_params=pltpu.CompilerParams(
            collective_id=0, has_side_effects=True, vmem_limit_bytes=54 * 1024 * 1024
        ),
    )(tokens, norm_gain.reshape(1, width), w_gate, w_up, w_down, routing.T, gate_weight.T)


def solution(mesh):
    placed = (
        P(("ep", "tp"), None),
        P(),
        P(("ep", "tp"), None, None),
        P(("ep", "tp"), None, None),
        P(("ep", "tp"), None, None),
        P(("ep", "tp"), None),
        P(("ep", "tp"), None),
    )
    return jax.shard_map(
        local, mesh=mesh, in_specs=placed, out_specs=P(("ep", "tp"), None), check_vma=False
    )
```

time: 127 us -> 56 us (0.44)
  Pallas kernels: 0 us -> 53.9 us
  blocking collectives: 42.4 us -> 0 us
  waiting for transfers between devices: 30.4 us -> 0 us
  local copies, waits for them, and re-layouts: 29.2 us -> 1.88 us
  matrix products: 10.7 us -> 0 us
  other arithmetic: 8.86 us -> 0 us
  starting transfers between devices: 5.02 us -> 0 us
    pallas_call x0 -> x1, Pallas kernels: none -> 53.9 us  [local(): pl.pallas_call(kernel, out_shape=jax.ShapeDtypeStruct((count, width), BF1...]
    all_to_all x1 -> x0, blocking collectives: 42.4 us -> none  [local(): lax.all_to_all(outgoing, ('ep', 'tp'), split_axis=0, concat_axis=0, tiled...]
    all_to_all x1 -> x0, waiting for transfers between devices: 30.4 us -> none  [local(): lax.all_to_all(answered, ('ep', 'tp'), split_axis=0, concat_axis=0, tiled...]
    reshape x4 -> x0, local copies, waits for them, and re-layouts: 16.1 us -> none  [the longest x1 4.11 us: local(): answered = expert_out.reshape(arrived.shape)]
    dot_general x2 -> x0, matrix products: 10.7 us -> none  [the longest x1 6.22 us: local(): jnp.dot(hidden, w_down[0], preferred_element_type=jnp.float32)]
    gather x2 -> x0, local copies, waits for them, and re-layouts: 7.52 us -> none  [the longest x1 4.22 us: local(): picked = returned.reshape(experts * capacity, width)[position]]
    reduce_sum x3 -> x0, other arithmetic: 6.99 us -> none  [the longest x1 5.59 us: local(): combined = jnp.sum(gate_weight[:, :, None] * picked, axis=1)]
    all_to_all x1 -> x0, starting transfers between devices: 5.02 us -> none  [local(): lax.all_to_all(answered, ('ep', 'tp'), split_axis=0, concat_axis=0, tiled...]
  transfers between devices with their start and end apart: 1 -> 0, of which waited for: 1 -> 0; matrix products, arithmetic and copies ran while one was open for 0% -> 0% of each run, Pallas kernels for 0% -> 0%
where the time goes in v2:
time: 56 us; the launch traced here: 55.8 us
  Pallas kernels  53.9 us (96%)
  local copies, waits for them, and re-layouts  1.88 us (3%)
    pallas_call x1, Pallas kernels, local(): pl.pallas_call(kernel, out_shape=jax.ShapeDtypeStruct((count, width), BF1...  53.9 us
    unnamed x1, local copies, waits for them, and re-layouts  1.88 us

profile of v2, /device:TPU:1, one launch (start us, length us, event | category | flops | bytes accessed | tf_op | source)
XLA Modules:
  0.0 55.8 jit_solution(15609855017080663541)
XLA Ops:
  0.0 53.9 %shard_map.73 = bf16[128,2048]{1,0:T(8,128)(2,1)} custom-call(bf16[128,2048]{1,0:T(8,128)(2,1)} %tok_hbm.1, f32[1,2048]{1,0:T(1,128)} %bitcast.3, bf16[1,2048,512]{2,1,0:T(8,128)(2,1)} %wg_hbm.1, bf16[1,2048,512]{2,1,0:T(8,128)(2,1)} %wu_hbm.1, bf16[1,512,2048]{2,1,0:T(8,128)(2,1)} %wd_hbm.1, s32[2,128]{1,0:T(2,128)} %bitcast.4, f32[2,128]{1,0:T(2,128)} %bitcast.5), custom_call_target="tpu_custom_call" | custom-call | tf_op jit(solution)/shard_map/pallas_call | solution.py:329
  53.9 1.9 %copy.9 = bf16[128,2048]{1,0:T(8,128)(2,1)} copy(bf16[128,2048]{1,0:T(8,128)(2,1)} %shard_map.73) | data formatting | bytes 1048576

commit v3 on v2

--- a/solution.py
+++ b/solution.py
@@ -29,10 +29,12 @@
 BLOCK = CAP * QUART
 AGA, AGB, FWD, RS1, RS2A, RS2B = range(6)
 RIGHT, LEFT = 0, 1
+PIECES = 1
+NEAR = sum(COUNT[name] for name in DIRECT)
 SIZES = tuple(sorted(set(COUNT.values())))
 ORDER = (
-    "dE", "oD", "dA", "oB", "oC", "k", "fE", "gD", "fA", "mS", "gB", "fD", "gC", "fB", "mU", "fC",
-    "cD", "cB", "cC", "rB", "rC", "cA", "rD", "cE", "bB", "bC", "rA", "bD", "rE", "bA", "bE",
+    "dE", "oD", "dA", "oC", "oB", "k", "fE", "gD", "fA", "mS", "gC", "fD", "gB", "fC", "mU", "cD",
+    "fB", "cC", "cB", "rC", "rD", "rB", "cA", "bC", "cE", "bD", "bB", "rA", "rE",
 )
 
 
@@ -44,15 +46,32 @@
     return jnp.where(mask, 1.0, 0.0).astype(BF16)
 
 
-def kernel(tok_hbm, gain_hbm, wg_hbm, wu_hbm, wd_hbm, route_hbm, gw_hbm, out_ref,
-           tok_ref, gain_ref, route_ref, gw_ref, wg, wu, wd, stack, place, unplace, spreads, gathers, msgs, meta_out, xbuf, xmeta, mrows, gall,
-           rows, ybuf, cbuf, rs1, rs2, back, ret,
-           w_sem, y_send, y_recv, m_send, m_recv, x_send, x_recv, xm_send, xm_recv, b_send, b_recv):
+def here():
+    me = lax.axis_index("ep")
+    return me // 8, (me // 2) % 4, me % 2
+
+
+def slots_and_ranks(route_ref, tokens):
+    z, y, c = here()
+    group = route_ref[0:1, :] // 4
+    square = jnp.broadcast_to(group.astype(F32), (tokens, tokens))
+    earlier = (square.T == square) & (iota((tokens, tokens), 0) < iota((tokens, tokens), 1))
+    rank = jnp.sum(jnp.where(earlier, 1, 0), axis=0, keepdims=True)
+    rel = ((z + 4 - group // 8) % 4) * 4 + (y + 4 - (group // 2) % 4) % 4
+    pair = jnp.zeros_like(group)
+    for n, (dz, dy) in enumerate(PAIRS):
+        pair = pair + jnp.where(rel == dz * 4 + dy, n, 0)
+    return pair * 2 + (group + c) % 2, rank
+
+
+def kernel(tok_hbm, gain_hbm, wg_hbm, wu_hbm, wd_hbm, route_hbm, gw_hbm, ret,
+           tok_ref, gain_ref, route_ref, gw_ref, wg, wu, wd, stack, place, spreads, gathers, msgs, meta_out, xbuf, xmeta, mrows, gall,
+           rows, ybuf, cbuf, rs1, rs2, back,
+           w_sem, y_send, y_recv, m_send, m_recv, x_send, x_recv, xm_send, xm_recv, b_send, b_recv, p_recv, own_sem):
     tokens, width = tok_ref.shape
     part = width // QUART
-    me = lax.axis_index("ep")
     mx = lax.axis_index("tp")
-    z, y, c = me // 8, (me // 2) % 4, me % 2
+    z, y, c = here()
     right = {"tp": (mx + 1) % 4}
     left = {"tp": (mx + 3) % 4}
 
@@ -92,23 +111,8 @@
     for q in range(QUART):
         stack[q * tokens:(q + 1) * tokens, :] = normed[:, q * part:(q + 1) * part]
 
-    first = route_ref[0:1, :]
-    second = route_ref[1:2, :]
-    group = first // 4
-    square = jnp.broadcast_to(group.astype(F32), (tokens, tokens))
-    earlier = (square.T == square) & (iota((tokens, tokens), 0) < iota((tokens, tokens), 1))
-    rank = jnp.sum(jnp.where(earlier, 1, 0), axis=0, keepdims=True)
-
-    def slot_of(group):
-        rel = ((z + 4 - group // 8) % 4) * 4 + (y + 4 - (group // 2) % 4) % 4
-        pair = jnp.zeros_like(group)
-        for n, (dz, dy) in enumerate(PAIRS):
-            pair = pair + jnp.where(rel == dz * 4 + dy, n, 0)
-        return pair * 2 + (group + c) % 2
-
-    slot_row = slot_of(group)
+    slot_row, rank = slots_and_ranks(route_ref, tokens)
     pos_row = slot_row * CAP + rank
-    pos_col = jnp.broadcast_to(pos_row.astype(F32), (tokens, tokens)).T[:, 0:1].astype(I32)
 
     r = iota((SLOTS * BLOCK, tokens), 0)
     place_of_r = (r // BLOCK) * CAP + r % CAP
@@ -118,14 +122,15 @@
     msgs[...] = jnp.dot(place[...], stack[...], preferred_element_type=F32).astype(BF16).reshape(SLOTS, BLOCK, part)
     xbuf[0, 0] = msgs[0]
 
+    first, second = route_ref[0:1, :], route_ref[1:2, :]
     line = iota((128, tokens), 0)
     of_line = (jnp.where(first % 4 == line % 4, gw_ref[0:1, :], 0.0)
                + jnp.where(second % 4 == line % 4, gw_ref[1:2, :], 0.0))
-    of_line = jnp.where(rank == line // 4, of_line, 0.0)
-    chosen = jnp.where(iota((SLOTS, tokens), 0) == slot_row, 1.0, 0.0)
+    of_line = jnp.where((slot_row % 8) * CAP + rank == line // 4, of_line, 0.0)
+    chosen = jnp.where(iota((8, tokens), 0) == slot_row // 8, 1.0, 0.0)
     meta = lax.dot_general(chosen, of_line, (((1,), (1,)), ((), ())), preferred_element_type=F32, precision=HIGHEST)
-    for slot in range(SLOTS):
-        meta_out[0, slot] = meta[slot:slot + 1, :]
+    for n in range(SLOTS // 8):
+        meta_out[0, n] = meta[n:n + 1, :]
 
     with jax.named_scope("barrier"):
         pl.semaphore_wait(barrier, SLOTS + 2 + 2 * len(near))
@@ -146,8 +151,8 @@
     def send_over(name):
         for slot in slots_of(name):
             if slot:
-                n = NAMES.index(name)
-                remote(msgs.at[slot], xbuf.at[0, slot], y_send, y_recv.at[n], peer(slot, -1)).start()
+                n, upper = NAMES.index(name), int(slot >= START[name] + COUNT[name] // 2)
+                remote(msgs.at[slot], xbuf.at[0, slot], y_send, y_recv.at[upper, n], peer(slot, -1)).start()
 
     def send_direct(name):
         n = NAMES.index(name)
@@ -166,10 +171,6 @@
             a, b = iota((edge, edge), 0), iota((edge, edge), 1)
             spread[...] = onehot(((a % run) // CAP) * BLOCK + (a // run) * CAP + a % CAP == b)
             gather[...] = onehot(((b % run) // CAP) * BLOCK + (b // run) * CAP + b % CAP == a)
-        r = iota((tokens, SLOTS * BLOCK), 1)
-        hit = (r // BLOCK) * CAP + r % CAP == pos_col
-        for q in range(QUART):
-            unplace[q * tokens:(q + 1) * tokens, :] = onehot(hit & ((r // CAP) % QUART == q))
 
     def hop(side, src, dst, kind, name):
         return remote(src, dst, x_send.at[side], x_recv.at[side, kind, NAMES.index(name)], left if side else right)
@@ -190,17 +191,17 @@
         part_of = span(name, kind - RS2A)
         return hop(side, cbuf.at[1 if side else 3, part_of], rs2.at[side, part_of], kind, name)
 
-    def over_done(name):
-        first_slot = max(1, START[name])
-        src = xbuf.at[0, slice(first_slot, START[name] + COUNT[name])]
-        remote(src, src, y_send, y_recv.at[NAMES.index(name)], right).wait_recv()
+    def over_done(name, kind):
+        half_of = span(name, kind)
+        if half_of.stop > 1:
+            src = xbuf.at[0, slice(max(1, half_of.start), half_of.stop)]
+            remote(src, src, y_send, y_recv.at[kind, NAMES.index(name)], right).wait_recv()
 
     def start_gather(name):
-        over_done(name)
-        ag(RIGHT, AGA, name).start()
-        ag(LEFT, AGB, name).start()
-        ag(RIGHT, AGB, name).start()
-        ag(LEFT, AGA, name).start()
+        for kind in (AGA, AGB):
+            over_done(name, kind)
+            ag(RIGHT, kind, name).start()
+            ag(LEFT, kind, name).start()
 
     def forward(name):
         ag(RIGHT, AGA, name).wait_recv()
@@ -212,7 +213,7 @@
         for n, side in enumerate(sides):
             remote(meta_out.at[0], meta_out.at[n + 1], xm_send.at[n], xm_recv.at[n], side).wait_recv()
         for slot in range(1, SLOTS):
-            remote(meta_out.at[:, slot], xmeta.at[:, slot], m_send, m_recv, peer(slot, -1)).start()
+            remote(meta_out.at[:, slot // 8], xmeta.at[:, slot], m_send, m_recv, peer(slot, -1)).start()
 
     def meta_use():
         src = xmeta.at[:, slice(1, SLOTS)]
@@ -226,7 +227,7 @@
             n, col = iota((count * BLOCK, 4 * SLOTS), 0), iota((count * BLOCK, 4 * SLOTS), 1)
             source = (n // (count * CAP)) * SLOTS + at + (n % (count * CAP)) // CAP
             picked = jnp.dot(jnp.where(source == col, 1.0, 0.0), mrows[...], preferred_element_type=F32, precision=HIGHEST)
-            mine = (n % CAP) * 4 + mx == col
+            mine = ((at + (n % (count * CAP)) // CAP) % 8) * 16 + (n % CAP) * 4 + mx == col
             gall[at * BLOCK:(at + count) * BLOCK, :] = jnp.broadcast_to(
                 jnp.sum(jnp.where(mine, picked, 0.0), axis=1, keepdims=True), (count * BLOCK, 128))
 
@@ -237,7 +238,8 @@
         spread, gather = spreads[SIZES.index(count)], gathers[SIZES.index(count)]
         edge, run, total_rows = 2 * count * BLOCK, 2 * count * CAP, 4 * count * CAP
         if name in DIRECT:
-            over_done(name)
+            over_done(name, AGA)
+            over_done(name, AGB)
         ag(RIGHT, AGB, name).wait_recv()
         ag(LEFT, AGA, name).wait_recv()
         fwd(RIGHT, name).wait_recv()
@@ -269,15 +271,33 @@
             if pair == 1:
                 rs_first(RIGHT, name).start()
                 rs_first(LEFT, name).start()
-        rs_second(RIGHT, RS2B, name).start()
-        rs_second(LEFT, RS2A, name).start()
+        if name in DIRECT:
+            to_source(name, RIGHT, AGB)
+            to_source(name, LEFT, AGA)
+            for slot in slots_of(name):
+                if slot:
+                    remote(cbuf.at[0, slot], ret.at[slot], b_send, b_recv, peer(slot, 1)).start()
+                else:
+                    pltpu.make_async_copy(cbuf.at[0, slot], ret.at[slot], own_sem).start()
+        else:
+            rs_second(RIGHT, RS2B, name).start()
+            rs_second(LEFT, RS2A, name).start()
+
+    def to_source(name, side, kind):
+        half_of = span(name, kind)
+        for slot in range(half_of.start, half_of.stop):
+            remote(cbuf.at[1 if side else 3, slot], ret.at[SLOTS + side * NEAR + slot], x_send.at[side], p_recv,
+                   peer(slot, 1, -1 if side else 1)).start()
 
     def reduce_first(name):
         for side, held, kind in ((RIGHT, 3, RS2A), (LEFT, 1, RS2B)):
             rs_first(side, name).wait_recv()
             mine = span(name, side)
             cbuf[held, mine] = (cbuf[held, mine].astype(F32) + rs1[mine].astype(F32)).astype(BF16)
-            rs_second(side, kind, name).start()
+            if name in DIRECT:
+                to_source(name, side, side)
+            else:
+                rs_second(side, kind, name).start()
 
     def give_back(name):
         for side in (RIGHT, LEFT):
@@ -287,10 +307,7 @@
         total = cbuf[0, all_of].astype(F32) + rs2[RIGHT, all_of].astype(F32) + rs2[LEFT, all_of].astype(F32)
         back[all_of] = total.astype(BF16)
         for slot in slots_of(name):
-            if slot:
-                remote(back.at[slot], ret.at[slot], b_send, b_recv, peer(slot, 1)).start()
-            else:
-                ret[0] = back[0]
+            remote(back.at[slot], ret.at[slot], b_send, b_recv, peer(slot, 1)).start()
 
     steps = {"d": send_direct, "g": start_gather, "f": forward, "c": compute, "r": reduce_first, "b": give_back, "o": send_over}
     plain = {"k": constants, "mS": meta_send, "mU": meta_use}
@@ -300,22 +317,57 @@
 
     with jax.named_scope("sent"):
         src = msgs.at[slice(1, SLOTS)]
-        remote(src, src, y_send, y_recv.at[0], right).wait_send()
+        remote(src, src, y_send, y_recv.at[0, 0], right).wait_send()
         for side in (RIGHT, LEFT):
             src = xbuf.at[slice(0, 3)]
             remote(src, src, x_send.at[side], x_recv.at[0, 0, 0], right).wait_send()
-        src = meta_out.at[:, slice(1, SLOTS)]
+        src = xmeta.at[:, slice(1, SLOTS)]
         remote(src, src, m_send, m_recv, right).wait_send()
         for n in range(3):
             remote(meta_out.at[0], meta_out.at[1], xm_send.at[n], xm_recv.at[n], right).wait_send()
     with jax.named_scope("back"):
         src = ret.at[slice(1, SLOTS)]
         remote(src, src, b_send, b_recv, right).wait_recv()
-    with jax.named_scope("final"):
-        result = jnp.dot(unplace[...], ret[...].reshape(SLOTS * BLOCK, part), preferred_element_type=F32).astype(BF16)
+        src = ret.at[slice(SLOTS, SLOTS + 2 * NEAR)]
+        remote(src, src, b_send, p_recv, right).wait_recv()
+        pltpu.make_async_copy(cbuf.at[0, 0], ret.at[0], own_sem).wait()
+        src = xbuf.at[0, slice(1, SLOTS)]
+        remote(src, src, b_send, b_recv, right).wait_send()
+
+
+def finish(ret_hbm, route_hbm, out_hbm, ret, route_ref, unplace, out, in_sem, out_sem):
+    tokens = route_ref.shape[1]
+    part = ret.shape[2]
+    piece = part // PIECES
+    fetch = [pltpu.make_async_copy(route_hbm, route_ref, in_sem.at[PIECES])]
+    for n in range(PIECES):
+        columns = slice(n * piece, (n + 1) * piece)
+        fetch.append(pltpu.make_async_copy(ret_hbm.at[:, :, columns], ret.at[:, :, columns], in_sem.at[n]))
+    for copy in fetch:
+        copy.start()
+    fetch[0].wait()
+    slot_row, rank = slots_and_ranks(route_ref, tokens)
+    pos_col = jnp.broadcast_to((slot_row * CAP + rank).astype(F32), (tokens, tokens)).T[:, 0:1].astype(I32)
+    r = iota((tokens, SLOTS * BLOCK), 1)
+    hit = (r // BLOCK) * CAP + r % CAP == pos_col
+    for q in range(QUART):
+        unplace[q * tokens:(q + 1) * tokens, :] = onehot(hit & ((r // CAP) % QUART == q))
+    copies = []
+    for n in range(PIECES):
+        fetch[1 + n].wait()
+        columns = slice(n * piece, (n + 1) * piece)
+        near, near_left = slice(SLOTS, SLOTS + NEAR), slice(SLOTS + NEAR, SLOTS + 2 * NEAR)
+        total = (ret[0:NEAR, :, columns].astype(F32) + ret[near, :, columns].astype(F32)
+                 + ret[near_left, :, columns].astype(F32))
+        stacked = jnp.concatenate([total.astype(BF16), ret[NEAR:SLOTS, :, columns]], axis=0)
+        row = jnp.dot(unplace[...], stacked.reshape(SLOTS * BLOCK, piece), preferred_element_type=F32).astype(BF16)
         for q in range(QUART):
-            out_ref[:, q * part:(q + 1) * part] = result[q * tokens:(q + 1) * tokens]
-        remote(src, src, b_send, b_recv, right).wait_send()
+            to = slice(q * part + n * piece, q * part + (n + 1) * piece)
+            out[:, to] = row[q * tokens:(q + 1) * tokens]
+            copies.append(pltpu.make_async_copy(out.at[:, to], out_hbm.at[:, to], out_sem.at[n, q]))
+            copies[-1].start()
+    for copy in copies:
+        copy.wait()
 
 
 def local(tokens, norm_gain, w_gate, w_up, w_down, routing, gate_weight):
@@ -323,14 +375,13 @@
     hidden = w_gate.shape[2]
     part = width // QUART
     total = SLOTS * BLOCK
-    vmem = pl.BlockSpec(memory_space=pltpu.VMEM)
     hbm = pl.BlockSpec(memory_space=pltpu.HBM)
     dma = pltpu.SemaphoreType.DMA
-    return pl.pallas_call(
+    returned = pl.pallas_call(
         kernel,
-        out_shape=jax.ShapeDtypeStruct((count, width), BF16),
+        out_shape=jax.ShapeDtypeStruct((SLOTS + 2 * NEAR, BLOCK, part), BF16),
         in_specs=[hbm] * 7,
-        out_specs=vmem,
+        out_specs=hbm,
         scratch_shapes=[
             pltpu.VMEM((count, width), BF16),
             pltpu.VMEM((1, width), F32),
@@ -341,11 +392,10 @@
             pltpu.VMEM((hidden, width), BF16),
             pltpu.VMEM((QUART * count, part), BF16),
             pltpu.VMEM((total, QUART * count), BF16),
-            pltpu.VMEM((QUART * count, total), BF16),
             [pltpu.VMEM((2 * size * BLOCK, 2 * size * BLOCK), BF16) for size in SIZES],
             [pltpu.VMEM((2 * size * BLOCK, 2 * size * BLOCK), BF16) for size in SIZES],
             pltpu.VMEM((SLOTS, BLOCK, part), BF16),
-            pltpu.VMEM((4, SLOTS, 1, 128), F32),
+            pltpu.VMEM((4, SLOTS // 8, 1, 128), F32),
             pltpu.VMEM((4, SLOTS, BLOCK, part), BF16),
             pltpu.VMEM((4, SLOTS, 1, 128), F32),
             pltpu.VMEM((4 * SLOTS, 128), F32),
@@ -356,14 +406,27 @@
             pltpu.VMEM((SLOTS, BLOCK, part), BF16),
             pltpu.VMEM((2, SLOTS, BLOCK, part), BF16),
             pltpu.VMEM((SLOTS, BLOCK, part), BF16),
-            pltpu.VMEM((SLOTS, BLOCK, part), BF16),
-            dma((7,)), dma, dma((len(NAMES),)), dma, dma,
-            dma((2,)), dma((2, 6, len(NAMES))), dma((3,)), dma((3,)), dma, dma,
+            dma((7,)), dma, dma((2, len(NAMES))), dma, dma,
+            dma((2,)), dma((2, 6, len(NAMES))), dma((3,)), dma((3,)), dma, dma, dma, dma,
         ],
         compiler_params=pltpu.CompilerParams(
             collective_id=0, has_side_effects=True, vmem_limit_bytes=54 * 1024 * 1024
         ),
     )(tokens, norm_gain.reshape(1, width), w_gate, w_up, w_down, routing.T, gate_weight.T)
+    return pl.pallas_call(
+        finish,
+        out_shape=jax.ShapeDtypeStruct((count, width), BF16),
+        in_specs=[hbm] * 2,
+        out_specs=hbm,
+        scratch_shapes=[
+            pltpu.VMEM((SLOTS + 2 * NEAR, BLOCK, part), BF16),
+            pltpu.VMEM((2, count), I32),
+            pltpu.VMEM((QUART * count, total), BF16),
+            pltpu.VMEM((count, width), BF16),
+            dma((PIECES + 1,)), dma((PIECES, QUART)),
+        ],
+        compiler_params=pltpu.CompilerParams(vmem_limit_bytes=54 * 1024 * 1024),
+    )(returned, routing.T)
 
 
 def solution(mesh):

time: 56 us -> 53.3 us (0.952)
  local copies, waits for them, and re-layouts: 1.88 us -> 0 us
  Pallas kernels: 53.9 us -> 53.1 us
    unnamed x1 -> x0, local copies, waits for them, and re-layouts: 1.88 us -> none
    pallas_call x1 -> x2, Pallas kernels: 53.9 us -> 53.1 us  [the longest x1 50.7 us: local(): pl.pallas_call(kernel, out_shape=jax.ShapeDtypeStruct((SLOTS + 2 * NEAR,...]
where the time goes in v3:
time: 53.3 us; the launch traced here: 53.1 us
  Pallas kernels  53.1 us (100%)
    pallas_call x1, Pallas kernels, local(): pl.pallas_call(kernel, out_shape=jax.ShapeDtypeStruct((SLOTS + 2 * NEAR,...  50.7 us
    pallas_call x1, Pallas kernels, local(): pl.pallas_call(finish, out_shape=jax.ShapeDtypeStruct((count, width), BF1...  2.39 us

profile of v3, /device:TPU:1, one launch (start us, length us, event | category | flops | bytes accessed | tf_op | source)
XLA Modules:
  0.0 53.1 jit_solution(17326179399759976034)
XLA Ops:
  0.0 50.7 %shard_map.73.ret_hbm = bf16[52,16,512]{2,1,0:T(8,128)(2,1)} custom-call(bf16[128,2048]{1,0:T(8,128)(2,1)} %tok_hbm.1, f32[1,2048]{1,0:T(1,128)} %bitcast.3, bf16[1,2048,512]{2,1,0:T(8,128)(2,1)} %wg_hbm.1, bf16[1,2048,512]{2,1,0:T(8,128)(2,1)} %wu_hbm.1, bf16[1,512,2048]{2,1,0:T(8,128)(2,1)} %wd_hbm.1, s32[2,128]{1,0:T(2,128)} %bitcast.4, f32[2,128]{1,0:T(2,128)} %bitcast.6), custom_call_target="tpu_custom_call" | custom-call | tf_op jit(solution)/shard_map/pallas_call | solution.py:380
  50.7 2.4 %shard_map.74 = bf16[128,2048]{1,0:T(8,128)(2,1)} custom-call(bf16[52,16,512]{2,1,0:T(8,128)(2,1)} %shard_map.73.ret_hbm, s32[2,128]{1,0:T(2,128)} %bitcast.5), custom_call_target="tpu_custom_call" | custom-call | tf_op jit(solution)/shard_map/pallas_call | solution.py:416

commit v4 on v3

--- a/solution.py
+++ b/solution.py
@@ -14,8 +14,8 @@
 CHUNKS = {
     "E": ((0, 0),),
     "A": ((0, 1), (0, 3), (1, 0), (3, 0)),
+    "D": ((1, 1), (3, 3), (1, 3)),
     "B": ((2, 0), (2, 1), (0, 2), (1, 2)),
-    "D": ((1, 1), (3, 3), (1, 3)),
     "C": ((2, 2), (2, 3), (3, 2), (3, 1)),
 }
 NAMES = tuple(CHUNKS)
@@ -31,10 +31,11 @@
 RIGHT, LEFT = 0, 1
 PIECES = 1
 NEAR = sum(COUNT[name] for name in DIRECT)
+EARLY = START["B"]
 SIZES = tuple(sorted(set(COUNT.values())))
 ORDER = (
-    "dE", "oD", "dA", "oC", "oB", "k", "fE", "gD", "fA", "mS", "gC", "fD", "gB", "fC", "mU", "cD",
-    "fB", "cC", "cB", "rC", "rD", "rB", "cA", "bC", "cE", "bD", "bB", "rA", "rE",
+    "dE", "oD", "dA", "oC", "oB", "m", "k", "fE", "gD", "fA", "mS", "gC", "fD", "gB", "fC", "mU",
+    "cD", "fB", "cC", "cB", "rC", "rD", "rB", "cA", "bC", "cE", "bD", "bB", "rA", "rE",
 )
 
 
@@ -101,7 +102,16 @@
     for side in (right, {"tp": (mx + 2) % 4}, left):
         pl.semaphore_signal(barrier, inc=1, device_id=side, device_id_type=MESH)
 
-    for copy in small:
+    small[2].wait()
+    slot_row, rank = slots_and_ranks(route_ref, tokens)
+    pos_row = slot_row * CAP + rank
+
+    r = iota((SLOTS * BLOCK, tokens), 0)
+    hit = (r // BLOCK) * CAP + r % CAP == pos_row
+    for q in range(QUART):
+        place[:, q * tokens:(q + 1) * tokens] = onehot(hit & ((r // CAP) % QUART == q))
+
+    for copy in small[:2]:
         copy.wait()
     for copy in weights:
         copy.start()
@@ -111,26 +121,13 @@
     for q in range(QUART):
         stack[q * tokens:(q + 1) * tokens, :] = normed[:, q * part:(q + 1) * part]
 
-    slot_row, rank = slots_and_ranks(route_ref, tokens)
-    pos_row = slot_row * CAP + rank
-
-    r = iota((SLOTS * BLOCK, tokens), 0)
-    place_of_r = (r // BLOCK) * CAP + r % CAP
-    hit = place_of_r == pos_row
-    for q in range(QUART):
-        place[:, q * tokens:(q + 1) * tokens] = onehot(hit & ((r // CAP) % QUART == q))
-    msgs[...] = jnp.dot(place[...], stack[...], preferred_element_type=F32).astype(BF16).reshape(SLOTS, BLOCK, part)
+    def put_in_order(low, high):
+        block = jnp.dot(place[low * BLOCK:high * BLOCK, :], stack[...], preferred_element_type=F32)
+        msgs[low:high] = block.astype(BF16).reshape(high - low, BLOCK, part)
+
+    put_in_order(0, EARLY)
+    put_in_order(EARLY, SLOTS)
     xbuf[0, 0] = msgs[0]
-
-    first, second = route_ref[0:1, :], route_ref[1:2, :]
-    line = iota((128, tokens), 0)
-    of_line = (jnp.where(first % 4 == line % 4, gw_ref[0:1, :], 0.0)
-               + jnp.where(second % 4 == line % 4, gw_ref[1:2, :], 0.0))
-    of_line = jnp.where((slot_row % 8) * CAP + rank == line // 4, of_line, 0.0)
-    chosen = jnp.where(iota((8, tokens), 0) == slot_row // 8, 1.0, 0.0)
-    meta = lax.dot_general(chosen, of_line, (((1,), (1,)), ((), ())), preferred_element_type=F32, precision=HIGHEST)
-    for n in range(SLOTS // 8):
-        meta_out[0, n] = meta[n:n + 1, :]
 
     with jax.named_scope("barrier"):
         pl.semaphore_wait(barrier, SLOTS + 2 + 2 * len(near))
@@ -140,8 +137,19 @@
                                             device_id=device, device_id_type=MESH)
 
     sides = (right, {"tp": (mx + 2) % 4}, left)
-    for n, side in enumerate(sides):
-        remote(meta_out.at[0], meta_out.at[n + 1], xm_send.at[n], xm_recv.at[n], side).start()
+    def meta_make():
+        small[3].wait()
+        first, second = route_ref[0:1, :], route_ref[1:2, :]
+        line = iota((128, tokens), 0)
+        of_line = (jnp.where(first % 4 == line % 4, gw_ref[0:1, :], 0.0)
+                   + jnp.where(second % 4 == line % 4, gw_ref[1:2, :], 0.0))
+        of_line = jnp.where((slot_row % 8) * CAP + rank == line // 4, of_line, 0.0)
+        chosen = jnp.where(iota((8, tokens), 0) == slot_row // 8, 1.0, 0.0)
+        meta = lax.dot_general(chosen, of_line, (((1,), (1,)), ((), ())), preferred_element_type=F32, precision=HIGHEST)
+        for n in range(SLOTS // 8):
+            meta_out[0, n] = meta[n:n + 1, :]
+        for n, side in enumerate(sides):
+            remote(meta_out.at[0], meta_out.at[n + 1], xm_send.at[n], xm_recv.at[n], side).start()
 
     def span(name, kind):
         first_slot, count = START[name], COUNT[name]
@@ -310,7 +318,7 @@
             remote(back.at[slot], ret.at[slot], b_send, b_recv, peer(slot, 1)).start()
 
     steps = {"d": send_direct, "g": start_gather, "f": forward, "c": compute, "r": reduce_first, "b": give_back, "o": send_over}
-    plain = {"k": constants, "mS": meta_send, "mU": meta_use}
+    plain = {"m": meta_make, "k": constants, "mS": meta_send, "mU": meta_use}
     for what in ORDER:
         with jax.named_scope(what):
             plain[what]() if what in plain else steps[what[0]](what[1])
@@ -338,11 +346,11 @@
 def finish(ret_hbm, route_hbm, out_hbm, ret, route_ref, unplace, out, in_sem, out_sem):
     tokens = route_ref.shape[1]
     part = ret.shape[2]
-    piece = part // PIECES
     fetch = [pltpu.make_async_copy(route_hbm, route_ref, in_sem.at[PIECES])]
+    piece = ret.shape[0] // PIECES
     for n in range(PIECES):
-        columns = slice(n * piece, (n + 1) * piece)
-        fetch.append(pltpu.make_async_copy(ret_hbm.at[:, :, columns], ret.at[:, :, columns], in_sem.at[n]))
+        some = slice(n * piece, (n + 1) * piece)
+        fetch.append(pltpu.make_async_copy(ret_hbm.at[some], ret.at[some], in_sem.at[n]))
     for copy in fetch:
         copy.start()
     fetch[0].wait()
@@ -352,20 +360,18 @@
     hit = (r // BLOCK) * CAP + r % CAP == pos_col
     for q in range(QUART):
         unplace[q * tokens:(q + 1) * tokens, :] = onehot(hit & ((r // CAP) % QUART == q))
+    for copy in fetch[1:]:
+        copy.wait()
+    total = ret[0:NEAR].astype(F32) + ret[SLOTS:SLOTS + NEAR].astype(F32) + ret[SLOTS + NEAR:].astype(F32)
+    ret[0:NEAR] = total.astype(BF16)
     copies = []
-    for n in range(PIECES):
-        fetch[1 + n].wait()
-        columns = slice(n * piece, (n + 1) * piece)
-        near, near_left = slice(SLOTS, SLOTS + NEAR), slice(SLOTS + NEAR, SLOTS + 2 * NEAR)
-        total = (ret[0:NEAR, :, columns].astype(F32) + ret[near, :, columns].astype(F32)
-                 + ret[near_left, :, columns].astype(F32))
-        stacked = jnp.concatenate([total.astype(BF16), ret[NEAR:SLOTS, :, columns]], axis=0)
-        row = jnp.dot(unplace[...], stacked.reshape(SLOTS * BLOCK, piece), preferred_element_type=F32).astype(BF16)
-        for q in range(QUART):
-            to = slice(q * part + n * piece, q * part + (n + 1) * piece)
-            out[:, to] = row[q * tokens:(q + 1) * tokens]
-            copies.append(pltpu.make_async_copy(out.at[:, to], out_hbm.at[:, to], out_sem.at[n, q]))
-            copies[-1].start()
+    for q in range(QUART):
+        row = jnp.dot(unplace[q * tokens:(q + 1) * tokens, :], ret[0:SLOTS].reshape(SLOTS * BLOCK, part),
+                      preferred_element_type=F32).astype(BF16)
+        columns = slice(q * part, (q + 1) * part)
+        out[:, columns] = row
+        copies.append(pltpu.make_async_copy(out.at[:, columns], out_hbm.at[:, columns], out_sem.at[q]))
+        copies[-1].start()
     for copy in copies:
         copy.wait()
 
@@ -423,7 +429,7 @@
             pltpu.VMEM((2, count), I32),
             pltpu.VMEM((QUART * count, total), BF16),
             pltpu.VMEM((count, width), BF16),
-            dma((PIECES + 1,)), dma((PIECES, QUART)),
+            dma((PIECES + 1,)), dma((QUART,)),
         ],
         compiler_params=pltpu.CompilerParams(vmem_limit_bytes=54 * 1024 * 1024),
     )(returned, routing.T)

time: 53.3 us -> 53 us (level)
  no operation moved by 1% of the time
where the time goes in v4:
time: 53 us; the launch traced here: 52.9 us
  Pallas kernels  52.9 us (100%)
    pallas_call x1, Pallas kernels, local(): pl.pallas_call(kernel, out_shape=jax.ShapeDtypeStruct((SLOTS + 2 * NEAR,...  50.5 us
    pallas_call x1, Pallas kernels, local(): pl.pallas_call(finish, out_shape=jax.ShapeDtypeStruct((count, width), BF1...  2.37 us

profile of v4, /device:TPU:1, one launch (start us, length us, event | category | flops | bytes accessed | tf_op | source)
XLA Modules:
  0.0 52.9 jit_solution(2665058218985045245)
XLA Ops:
  0.0 50.5 %shard_map.73.ret_hbm = bf16[52,16,512]{2,1,0:T(8,128)(2,1)} custom-call(bf16[128,2048]{1,0:T(8,128)(2,1)} %tok_hbm.1, f32[1,2048]{1,0:T(1,128)} %bitcast.3, bf16[1,2048,512]{2,1,0:T(8,128)(2,1)} %wg_hbm.1, bf16[1,2048,512]{2,1,0:T(8,128)(2,1)} %wu_hbm.1, bf16[1,512,2048]{2,1,0:T(8,128)(2,1)} %wd_hbm.1, s32[2,128]{1,0:T(2,128)} %bitcast.4, f32[2,128]{1,0:T(2,128)} %bitcast.6), custom_call_target="tpu_custom_call" | custom-call | tf_op jit(solution)/shard_map/pallas_call | solution.py:386
  50.5 2.4 %shard_map.74 = bf16[128,2048]{1,0:T(8,128)(2,1)} custom-call(bf16[52,16,512]{2,1,0:T(8,128)(2,1)} %shard_map.73.ret_hbm, s32[2,128]{1,0:T(2,128)} %bitcast.5), custom_call_target="tpu_custom_call" | custom-call | tf_op jit(solution)/shard_map/pallas_call | solution.py:422

commit v5 on v4

--- a/solution.py
+++ b/solution.py
@@ -15,8 +15,8 @@
     "E": ((0, 0),),
     "A": ((0, 1), (0, 3), (1, 0), (3, 0)),
     "D": ((1, 1), (3, 3), (1, 3)),
-    "B": ((2, 0), (2, 1), (0, 2), (1, 2)),
-    "C": ((2, 2), (2, 3), (3, 2), (3, 1)),
+    "B": ((0, 2), (2, 0), (3, 1), (1, 2)),
+    "C": ((2, 2), (2, 1), (2, 3), (3, 2)),
 }
 NAMES = tuple(CHUNKS)
 DIRECT = "EA"

time: 53 us -> 52.5 us (level)
  no operation moved by 1% of the time
where the time goes in v5:
time: 52.5 us; the launch traced here: 52.4 us
  Pallas kernels  52.4 us (100%)
    pallas_call x1, Pallas kernels, local(): pl.pallas_call(kernel, out_shape=jax.ShapeDtypeStruct((SLOTS + 2 * NEAR,...  50 us
    pallas_call x1, Pallas kernels, local(): pl.pallas_call(finish, out_shape=jax.ShapeDtypeStruct((count, width), BF1...  2.37 us

profile of v5, /device:TPU:1, one launch (start us, length us, event | category | flops | bytes accessed | tf_op | source)
XLA Modules:
  0.0 52.4 jit_solution(167674203956129218)
XLA Ops:
  0.0 50.0 %shard_map.73.ret_hbm = bf16[52,16,512]{2,1,0:T(8,128)(2,1)} custom-call(bf16[128,2048]{1,0:T(8,128)(2,1)} %tok_hbm.1, f32[1,2048]{1,0:T(1,128)} %bitcast.3, bf16[1,2048,512]{2,1,0:T(8,128)(2,1)} %wg_hbm.1, bf16[1,2048,512]{2,1,0:T(8,128)(2,1)} %wu_hbm.1, bf16[1,512,2048]{2,1,0:T(8,128)(2,1)} %wd_hbm.1, s32[2,128]{1,0:T(2,128)} %bitcast.4, f32[2,128]{1,0:T(2,128)} %bitcast.6), custom_call_target="tpu_custom_call" | custom-call | tf_op jit(solution)/shard_map/pallas_call | solution.py:386
  50.0 2.4 %shard_map.74 = bf16[128,2048]{1,0:T(8,128)(2,1)} custom-call(bf16[52,16,512]{2,1,0:T(8,128)(2,1)} %shard_map.73.ret_hbm, s32[2,128]{1,0:T(2,128)} %bitcast.5), custom_call_target="tpu_custom_call" | custom-call | tf_op jit(solution)/shard_map/pallas_call | solution.py:422

commit v6 on v5

--- a/solution.py
+++ b/solution.py
@@ -35,7 +35,7 @@
 SIZES = tuple(sorted(set(COUNT.values())))
 ORDER = (
     "dE", "oD", "dA", "oC", "oB", "m", "k", "fE", "gD", "fA", "mS", "gC", "fD", "gB", "fC", "mU",
-    "cD", "fB", "cC", "cB", "rC", "rD", "rB", "cA", "bC", "cE", "bD", "bB", "rA", "rE",
+    "cD", "fB", "cC", "cB", "rC", "rB", "rD", "cA", "bC", "cE", "bB", "bD", "rA", "rE",
 )
 
 

time: 52.5 us -> 52.6 us (level)
  no operation moved by 1% of the time
where the time goes in v6:
time: 52.6 us; the launch traced here: 52.5 us
  Pallas kernels  52.5 us (100%)
    pallas_call x1, Pallas kernels, local(): pl.pallas_call(kernel, out_shape=jax.ShapeDtypeStruct((SLOTS + 2 * NEAR,...  50.1 us
    pallas_call x1, Pallas kernels, local(): pl.pallas_call(finish, out_shape=jax.ShapeDtypeStruct((count, width), BF1...  2.37 us

profile of v6, /device:TPU:1, one launch (start us, length us, event | category | flops | bytes accessed | tf_op | source)
XLA Modules:
  0.0 52.5 jit_solution(17126048165953683379)
XLA Ops:
  0.0 50.1 %shard_map.73.ret_hbm = bf16[52,16,512]{2,1,0:T(8,128)(2,1)} custom-call(bf16[128,2048]{1,0:T(8,128)(2,1)} %tok_hbm.1, f32[1,2048]{1,0:T(1,128)} %bitcast.3, bf16[1,2048,512]{2,1,0:T(8,128)(2,1)} %wg_hbm.1, bf16[1,2048,512]{2,1,0:T(8,128)(2,1)} %wu_hbm.1, bf16[1,512,2048]{2,1,0:T(8,128)(2,1)} %wd_hbm.1, s32[2,128]{1,0:T(2,128)} %bitcast.4, f32[2,128]{1,0:T(2,128)} %bitcast.6), custom_call_target="tpu_custom_call" | custom-call | tf_op jit(solution)/shard_map/pallas_call | solution.py:386
  50.1 2.4 %shard_map.74 = bf16[128,2048]{1,0:T(8,128)(2,1)} custom-call(bf16[52,16,512]{2,1,0:T(8,128)(2,1)} %shard_map.73.ret_hbm, s32[2,128]{1,0:T(2,128)} %bitcast.5), custom_call_target="tpu_custom_call" | custom-call | tf_op jit(solution)/shard_map/pallas_call | solution.py:422
